TPU v7x, 128 devices: a whole 4x4x4 slice. The times are simulated.
128 devices in a mesh: fs: 16 (over z, y), rep: 4 (over x), tp: 2 (over core).
Axes of the slice: x: 4, y: 4, z: 4, core: 2. Of those that a mesh axis runs over, the one named last changes fastest.
Arguments:
- saved_latent: bfloat16 [49152, 2048], P(('fs', 'rep')), may hold values from -6 to 6
- query_cotangent: bfloat16 [49152, 3072], P(('fs', 'rep'), 'tp'), may hold values from -6 to 6
- mix_cotangent: bfloat16 [49152, 4096], P(('fs', 'rep')), may hold values from -6 to 6
- head_outputs: bfloat16 [49152, 2048], P(('fs', 'rep'), 'tp'), may hold values from -6 to 6
- query_weight: float32 [2048, 3072], P('fs', 'tp'), may hold values from -0.125 to 0.125
- out_weight: float32 [4096, 2048], P('fs', 'tp'), may hold values from -0.125 to 0.125
- query_basis: bfloat16 [2048, 256], replicated, may hold values from -0.125 to 0.125
- out_basis: bfloat16 [4096, 256], replicated, may hold values from -0.09375 to 0.09375
- query_mean: float32 [256, 3072], P('fs', 'tp'), may hold values from -3 to 3
- query_var: float32 [256, 3072], P('fs', 'tp'), may hold values from 0.1 to 1
- out_mean: float32 [256, 2048], P('fs', 'tp'), may hold values from -3 to 3
- out_var: float32 [256, 2048], P('fs', 'tp'), may hold values from 0.1 to 1
Outputs:
- query_step: float32 [2048, 3072], P('fs', 'tp')
- out_step: float32 [4096, 2048], P('fs', 'tp')
- query_copy: bfloat16 [2048, 3072], P('fs', 'tp')
- out_copy: bfloat16 [4096, 2048], P('fs', 'tp')
All inputs are finite; a program needn't handle non-finite values.
Results may differ from a plain program's by a relative error of at most 0.001.
Values sent between devices are 32-bit elements; how exact they have to be, the bound alone decides.
No kernel may reach another device: no remote copies, remote signals or barrier semaphores. Data moves between devices by JAX's collectives and lax.ppermute only.
A program may use at most 128 MiB of HBM per device.

v0:
```python
import jax
import jax.numpy as jnp
from jax import lax
from jax.sharding import PartitionSpec as P


def split_up(value, dim, devices):
    dims = value.shape
    tiles = value.reshape(*dims[:dim], devices, dims[dim] // devices, *dims[dim + 1 :])
    return jnp.moveaxis(tiles, dim, 0)


def sent_and_summed(value, axis, dim):
    devices = lax.axis_size(axis)
    tiles = lax.all_to_all(split_up(value, dim, devices), axis, 0, 0, tiled=True)
    return jnp.sum(tiles, axis=0)


def side_by_side(arrays, axis, dim, along):
    widths = [a.shape[along] for a in arrays]
    both = jnp.concatenate(arrays, axis=along)
    whole = sent_and_summed(both, axis, dim)
    return tuple(jnp.split(whole, [sum(widths[:k]) for k in range(1, len(widths))], axis=along))


def copy_for_each(value, axis):
    copies = jnp.broadcast_to(value, (lax.axis_size(axis), *value.shape))
    return lax.all_to_all(copies, axis, split_axis=0, concat_axis=0, tiled=True)


def over_copies(value, axis):
    everything = copy_for_each(value, axis)
    return jnp.sum(everything, axis=0)


def packed_total(arrays, axis):
    ravelled, at, finished = (jnp.concatenate([a.reshape(-1) for a in arrays]), 0, [])
    running = over_copies(ravelled, axis)
    for a in arrays:
        finished.append(running[at : at + a.size].reshape(a.shape))
        at += a.size
    return tuple(finished)


def in_one_piece(arrays, axis, dim, along):
    ends, at = ([], 0)
    for a in arrays[:-1]:
        at += a.shape[along]
        ends.append(at)
    both = jnp.concatenate(arrays, axis=along)
    return tuple(jnp.split(lax.all_gather(both, axis, axis=dim, tiled=True), ends, axis=along))


def token_sum(left, right):
    return lax.dot_general(
        left, right, (((0,), (0,)), ((), ())), preferred_element_type=jnp.float32
    )


def project(basis, grad):
    return lax.dot_general(
        basis.astype(jnp.float32), grad, (((0,), (0,)), ((), ())), precision=lax.Precision.HIGHEST
    )


def moment_direction(proj, scale, mean, var):
    scaled = scale * proj
    new_mean = 0.8 * mean + 0.2 * scaled
    new_var = 0.9 * var + 0.1 * scaled * scaled
    return new_mean / jnp.sqrt(new_var)


def on_device(
    saved_latent,
    query_cotangent,
    mix_cotangent,
    head_outputs,
    query_weight,
    out_weight,
    query_basis,
    out_basis,
    query_mean,
    query_var,
    out_mean,
    out_var,
):
    query_rows = query_weight.shape[0]
    out_rows = out_weight.shape[0]
    position = lax.axis_index("fs")
    query_local = lax.dynamic_slice_in_dim(query_basis, position * query_rows, query_rows, 0)
    out_local = lax.dynamic_slice_in_dim(out_basis, position * out_rows, out_rows, 0)
    query_early = project(query_basis, token_sum(saved_latent, query_cotangent))
    out_early = project(out_basis, token_sum(mix_cotangent, head_outputs))
    query_shard, out_shard = side_by_side((query_early, out_early), "fs", 0, 1)
    query_proj, out_proj = packed_total((query_shard, out_shard), "rep")
    query_squares, out_squares = packed_total(
        (jnp.sum(query_proj * query_proj), jnp.sum(out_proj * out_proj)), ("fs", "tp")
    )
    spread = lax.axis_size("fs") * lax.axis_size("tp")
    query_count = float(query_proj.shape[0] * query_proj.shape[1] * spread)
    out_count = float(out_proj.shape[0] * out_proj.shape[1] * spread)
    query_scale = 1.0 / jnp.maximum(jnp.sqrt(query_squares / query_count), 1.0)
    out_scale = 1.0 / jnp.maximum(jnp.sqrt(out_squares / out_count), 1.0)
    query_dir = moment_direction(query_proj, query_scale, query_mean, query_var)
    out_dir = moment_direction(out_proj, out_scale, out_mean, out_var)
    query_left = query_local.astype(jnp.float32)
    out_left = out_local.astype(jnp.float32)
    pieces = in_one_piece((query_dir, out_dir), "fs", 0, 1)
    query_step = jnp.dot(query_left, pieces[0], precision=lax.Precision.HIGHEST)
    out_step = jnp.dot(out_left, pieces[1], precision=lax.Precision.HIGHEST)
    query_copy = (query_weight - 0.05 * query_step).astype(jnp.bfloat16)
    out_copy = (out_weight - 0.05 * out_step).astype(jnp.bfloat16)
    return (query_step, out_step, query_copy, out_copy)


def solution(mesh):
    placed = (
        P(("fs", "rep"), None),
        P(("fs", "rep"), "tp"),
        P(("fs", "rep"), None),
        P(("fs", "rep"), "tp"),
        P("fs", "tp"),
        P("fs", "tp"),
        P(),
        P(),
        P("fs", "tp"),
        P("fs", "tp"),
        P("fs", "tp"),
        P("fs", "tp"),
    )
    return jax.shard_map(
        on_device,
        mesh=mesh,
        in_specs=placed,
        out_specs=(P("fs", "tp"), P("fs", "tp"), P("fs", "tp"), P("fs", "tp")),
        check_vma=False,
    )
```

profile of v0, /device:TPU:0, one launch (start us, length us, event | category | flops | bytes accessed | tf_op | source)
XLA Modules:
  0.0 184.6 jit_solution(17855957719749976158)
XLA Ops:
  7.2 0.0 all-gather.2.cloned.1.call-start
  7.2 9.7 %fusion.16 = f32[4096,1024]{1,0:T(8,128)S(1)} fusion(bf16[768,4096]{1,0:T(8,128)(2,1)} %param.14, bf16[768,1024]{1,0:T(8,128)(2,1)} %param.15), kind=kOutput, calls=%fused_computation.31 | convolution fusion | flops 6442450944 | bytes 24641536 | tf_op jit(solution)/shard_map/dot_general | solution.py:55
  16.9 13.3 %convolution_bitcast_fusion.1 = f32[256,1024]{0,1:T(8,128)S(1)} fusion(f32[4096,1024]{1,0:T(8,128)S(1)} %fusion.16, bf16[4096,256]{1,0:T(8,128)(2,1)S(1)} %copy-done.2), kind=kOutput, calls=%fused_computation.4 | convolution fusion | flops 12884901888 | bytes 19922944 | tf_op jit(solution)/shard_map/dot_general | solution.py:61
  30.3 5.1 %fusion.15 = f32[2048,1536]{1,0:T(8,128)S(1)} fusion(bf16[768,2048]{1,0:T(8,128)(2,1)S(1)} %copy-done, bf16[768,1536]{1,0:T(8,128)(2,1)S(1)} %copy-done.5), kind=kOutput, calls=%fused_computation.30 | convolution fusion | flops 4831838208 | bytes 18087936 | tf_op jit(solution)/shard_map/dot_general | solution.py:55
  35.5 10.6 %convolution_bitcast_fusion = f32[256,1536]{0,1:T(8,128)S(1)} fusion(f32[2048,1536]{1,0:T(8,128)S(1)} %fusion.15, bf16[2048,256]{1,0:T(8,128)(2,1)S(1)} %copy-done.3), kind=kOutput, calls=%fused_computation | convolution fusion | flops 9663676416 | bytes 15204352 | tf_op jit(solution)/shard_map/dot_general | solution.py:61
  46.1 1.7 pad_maximum_fusion
  47.8 3.2 %copy.18 = f32[256,2560]{1,0:T(8,128)} copy(f32[256,2560]{0,1:T(8,128)} %pad_maximum_fusion) | data formatting | bytes 5242880 | tf_op jit(solution)/shard_map/concatenate | solution.py:21
  51.0 42.3 %all_to_all.17 = f32[16,16,2560]{2,1,0:T(8,128)} all-to-all(f32[16,16,2560]{2,1,0:T(8,128)} %bitcast.20), channel_id=1, replica_groups=mesh['fs'=16,'rep'=4,'tp'=2] {'fs'}, dimensions={0} | all-to-all | bytes 5242880 | tf_op jit(solution)/shard_map/all_to_all | solution.py:15
  93.3 1.9 %reduce_sum.45 = f32[16,2560]{1,0:T(8,128)S(1)} reduce(f32[16,16,2560]{2,1,0:T(8,128)} %all_to_all.17, f32[]{:T(128)} %constant.12.clone.1), dimensions={0}, to_apply=%region_0.0 | reduce | flops 614400 | bytes 2785284 | tf_op jit(solution)/shard_map/reduce_sum | solution.py:16
  95.2 0.3 broadcast_in_dim.6
  95.6 13.7 %all_to_all.18 = f32[4,1,40960]{2,1,0:T(1,128)} all-to-all(f32[4,1,40960]{2,1,0:T(1,128)S(1)} %broadcast_in_dim.6), channel_id=1, replica_groups=mesh['fs'=16,'rep'=4,'tp'=2] {'rep'}, dimensions={0} | all-to-all | bytes 1310720 | tf_op jit(solution)/shard_map/all_to_all | solution.py:28
  109.3 1.7 reduce_sum.46
  111.0 0.6 multiply_reduce_fusion
  111.6 0.6 multiply_reduce_fusion.1
  112.2 1.4 pad_maximum_fusion.3
  113.6 11.2 %all_to_all.19 = f32[32,1,2]{2,1,0:T(1,128)S(1)} all-to-all(f32[32,1,2]{2,1,0:T(1,128)S(1)} %broadcast_in_dim.7), channel_id=1, replica_groups=mesh['fs'=16,'rep'=4,'tp'=2] {'fs','tp'}, dimensions={0} | all-to-all | bytes 512 | tf_op jit(solution)/shard_map/all_to_all | solution.py:28
  124.8 0.1 reduce_sum.49
  124.9 0.6 fusion.14
  127.0 1.0 fusion.7
  128.0 0.9 fusion.10
  128.9 0.7 pad_maximum_fusion.2
  129.6 42.1 %all-gather.2.cloned.1.call-done = f32[256,2560]{1,0:T(8,128)} async-done(((f32[16,2560]{1,0:T(8,128)}), f32[256,2560]{1,0:T(8,128)}) %all-gather.2.cloned.1.call-update) | async-done | bytes 2621456 | tf_op jit(solution)/shard_map/all_gather | solution.py:51
  171.7 3.6 %subtract_convert_fusion = (bf16[256,1024]{1,0:T(8,128)(2,1)}, f32[256,1024]{1,0:T(8,128)}) fusion(f32[256,1024]{1,0:T(8,128)} %param.17, f32[256,2560]{1,0:T(8,128)} %all-gather.2.cloned.1.call-done, bf16[4096,256]{1,0:T(8,128)(2,1)} %param.19, s32[]{:T(128)S(6)} %select_n.7), kind=kOutput, calls=%fused_computation.7 | convolution fusion | flops 806092800 | bytes 3801092 | tf_op jit(solution)/shard_map/dot_general | solution.py:110
  175.2 2.5 %subtract_convert_fusion.1 = (bf16[128,1536]{1,0:T(8,128)(2,1)}, f32[128,1536]{1,0:T(8,128)}) fusion(f32[128,1536]{1,0:T(8,128)S(1)} %copy-done.4, f32[256,2560]{1,0:T(8,128)S(1)} %copy-done.1, bf16[2048,256]{1,0:T(8,128)(2,1)} %param.18, s32[]{:T(128)S(6)} %select_n.6), kind=kOutput, calls=%fused_computation.8 | convolution fusion | flops 604569600 | bytes 3604484 | tf_op jit(solution)/shard_map/dot_general | solution.py:109
  (23 shorter events, 0.2 us)
Async XLA Ops:
  7.2 23.1 %copy-start = (bf16[768,2048]{1,0:T(8,128)(2,1)S(1)}, bf16[768,2048]{1,0:T(8,128)(2,1)}, u32[]{:S(2)}) copy-start(bf16[768,2048]{1,0:T(8,128)(2,1)} %param.12) | copy-start | bytes 9437188
  7.2 164.5 %all-gather.2.cloned.1.call-start = ((), (), s32[]{:S(2)}) async-start(), calls=%async_computation.3 | async-start | bytes 2785280 | tf_op jit(solution)/shard_map/all_gather | solution.py:51
  7.2 9.7 %copy-start.2 = (bf16[4096,256]{1,0:T(8,128)(2,1)S(1)}, bf16[4096,256]{1,0:T(8,128)(2,1)}, u32[]{:S(2)}) copy-start(bf16[4096,256]{1,0:T(8,128)(2,1)} %param.19) | copy-start | bytes 6291460
  16.9 13.4 %copy-start.5 = (bf16[768,1536]{1,0:T(8,128)(2,1)S(1)}, bf16[768,1536]{1,0:T(8,128)(2,1)}, u32[]{:S(2)}) copy-start(bf16[768,1536]{1,0:T(8,128)(2,1)} %param.13) | copy-start | bytes 7077892
  30.3 5.1 %copy-start.3 = (bf16[2048,256]{1,0:T(8,128)(2,1)S(1)}, bf16[2048,256]{1,0:T(8,128)(2,1)}, u32[]{:S(2)}) copy-start(bf16[2048,256]{1,0:T(8,128)(2,1)} %param.18) | copy-start | bytes 3145732
  171.7 3.6 %copy-start.1 = (f32[256,2560]{1,0:T(8,128)S(1)}, f32[256,2560]{1,0:T(8,128)}, u32[]{:S(2)}) copy-start(f32[256,2560]{1,0:T(8,128)} %all-gather.2.cloned.1.call-done) | copy-start | bytes 7864324
  171.7 3.6 %copy-start.4 = (f32[128,1536]{1,0:T(8,128)S(1)}, f32[128,1536]{1,0:T(8,128)}, u32[]{:S(2)}) copy-start(f32[128,1536]{1,0:T(8,128)} %param.16) | copy-start | bytes 2359300
Sparse Core Ops, SparseCore 0:
  129.7 41.9 all-gather.1
where the time goes:
time: 185 us
  blocking collectives  67.2 us (36%)
  matrix products  44.8 us (24%)
  waiting for transfers between devices  42.1 us (23%)
  between operations  15.7 us (8%)
  other arithmetic  10.5 us (6%)
  local copies, waits for them, and re-layouts  4.27 us (2%)
    all_to_all x1, blocking collectives, sent_and_summed(): lax.all_to_all(split_up(value, dim, devices), axis, 0, 0, tiled=True)  42.3 us
    all_gather x1, waiting for transfers between devices, in_one_piece(): lax.all_gather(both, axis, axis=dim, tiled=True)  42.1 us
    all_to_all x2, blocking collectives, copy_for_each(): return lax.all_to_all(copies, axis, split_axis=0, concat_axis=0, tiled=True)  24.9 us
    dot_general x2, matrix products, project(): lax.dot_general(basis.astype(jnp.float32), grad, (((0,), (0,)), ((), ()))...  23.9 us
    dot_general x2, matrix products, token_sum(): lax.dot_general(left, right, (((0,), (0,)), ((), ())), preferred_element_...  14.8 us
  transfers between devices with their start and end apart: 1, of which 1 were waited for; matrix products, arithmetic and copies ran while one was open for 0% of the time, Pallas kernels for 0%

commit v1 on v0

v1 whole, which is shorter than its diff:
```python
import functools

import jax
import jax.numpy as jnp
from jax import lax
from jax.experimental import pallas as pl
from jax.experimental.pallas import tpu as pltpu
from jax.sharding import PartitionSpec as P

F32 = jnp.float32
BF16 = jnp.bfloat16
STEPS = 3


def halves(value):
    high = value.astype(BF16)
    return high, (value - high.astype(F32)).astype(BF16)


def over_tokens(left, right):
    return lax.dot_general(left, right, (((0,), (0,)), ((), ())), preferred_element_type=F32)


def early_kernel(parts, rows, latent, cot, mix, heads, qbasis, obasis, out):
    step = pl.program_id(0)

    def one(tokens, basis, other, start):
        low_rank = jnp.dot(tokens[...], basis[...], preferred_element_type=F32)
        high, low = halves(low_rank)
        width = other.shape[1] // parts
        for part in range(parts):
            columns = other[:, part * width : (part + 1) * width]
            term = over_tokens(high, columns) + over_tokens(low, columns)
            term = term.reshape(term.shape[0] // rows, rows, width)
            spot = (slice(None), part, slice(None), slice(start, start + width))

            @pl.when(step == 0)
            def _():
                out[spot] = term

            @pl.when(step > 0)
            def _():
                out[spot] += term

    one(latent, qbasis, cot, 0)
    one(mix, obasis, heads, cot.shape[1] // parts)


def early(latent, cot, mix, heads, qbasis, obasis, blocks, parts):
    rows = qbasis.shape[1] // blocks
    wide = (cot.shape[1] + heads.shape[1]) // parts
    tokens = latent.shape[0] // STEPS
    moving = [pl.BlockSpec((tokens, a.shape[1]), lambda i: (i, 0)) for a in (latent, cot, mix, heads)]
    held = [pl.BlockSpec(a.shape, lambda i: (0, 0)) for a in (qbasis, obasis)]
    shape = (blocks, parts, rows, wide)
    return pl.pallas_call(
        functools.partial(early_kernel, parts, rows),
        grid=(STEPS,),
        in_specs=moving + held,
        out_specs=pl.BlockSpec(shape, lambda i: (0, 0, 0, 0)),
        out_shape=jax.ShapeDtypeStruct(shape, F32),
        compiler_params=pltpu.CompilerParams(vmem_limit_bytes=48 << 20),
        cost_estimate=pl.CostEstimate(flops=4_500_000_000, bytes_accessed=19_000_000, transcendentals=0),
        name="early",
    )(latent, cot, mix, heads, qbasis, obasis)


def lanes(value):
    return jnp.sum(value.reshape(value.shape[0], value.shape[1] // 128, 128), axis=(0, 1)).reshape(1, 128)


def total_kernel(split, copies, terms, proj, squares):
    step = pl.program_id(0)
    part = jnp.sum(terms[...], axis=0)

    @pl.when(step == 0)
    def _():
        proj[...] = part

    @pl.when(step > 0)
    def _():
        proj[...] += part

    @pl.when(step == pl.num_programs(0) - 1)
    def _():
        whole = proj[...]
        square = whole * whole
        mine = jnp.concatenate([lanes(square[:, :split]), lanes(square[:, split:])], axis=0)
        squares[...] = jnp.broadcast_to(mine, (copies, 2, 128))


def total(terms, split, copies):
    count, rows, wide = terms.shape
    chunk = count // 4
    return pl.pallas_call(
        functools.partial(total_kernel, split, copies),
        grid=(4,),
        in_specs=[pl.BlockSpec((chunk, rows, wide), lambda i: (i, 0, 0))],
        out_specs=[
            pl.BlockSpec((rows, wide), lambda i: (0, 0)),
            pl.BlockSpec((copies, 2, 128), lambda i: (0, 0, 0)),
        ],
        out_shape=[
            jax.ShapeDtypeStruct((rows, wide), F32),
            jax.ShapeDtypeStruct((copies, 2, 128), F32),
        ],
        name="total",
    )(terms)


def direction_kernel(split, counts, squares, proj, qmean, qvar, omean, ovar, out):
    sums = jnp.sum(jnp.sum(squares[...], axis=0), axis=1, keepdims=True)
    part = lax.axis_index("rep")

    def one(index, start, width, mean, var):
        spot = pl.ds(pl.multiple_of(part * width, 128), width)
        scale = 1.0 / jnp.maximum(jnp.sqrt(sums[index : index + 1] / counts[index]), 1.0)
        scaled = scale * proj[:, start : start + width]
        new_mean = 0.8 * mean[:, spot] + 0.2 * scaled
        new_var = 0.9 * var[:, spot] + 0.1 * scaled * scaled
        return new_mean / jnp.sqrt(new_var)

    wide = proj.shape[1]
    both = jnp.concatenate(
        [one(0, 0, split, qmean, qvar), one(1, split, wide - split, omean, ovar)], axis=1
    )
    out[...] = jnp.broadcast_to(both, out.shape)


def direction(squares, proj, qmean, qvar, omean, ovar, split, counts, copies):
    return pl.pallas_call(
        functools.partial(direction_kernel, split, counts),
        out_shape=jax.ShapeDtypeStruct((copies, *proj.shape), F32),
        name="direction",
    )(squares, proj, qmean, qvar, omean, ovar)


def late_kernel(split, dirs, qbasis, obasis, qweight, oweight, qstep, ostep, qcopy, ocopy):
    def one(basis, start, width, weight, step, copy):
        whole = dirs[:, 0, :, start : start + width]
        high, low = halves(whole.reshape(whole.shape[0] * whole.shape[1], width))
        value = jnp.dot(basis[...], high, preferred_element_type=F32)
        value += jnp.dot(basis[...], low, preferred_element_type=F32)
        step[...] = value
        copy[...] = (weight[...] - 0.05 * value).astype(BF16)

    one(qbasis, 0, split, qweight, qstep, qcopy)
    one(obasis, split, dirs.shape[3] - split, oweight, ostep, ocopy)


def late(dirs, qbasis, obasis, qweight, oweight, split):
    blocks, parts, rows, wide = dirs.shape
    qspec = pl.BlockSpec((qweight.shape[0], split), lambda i: (0, i))
    ospec = pl.BlockSpec((oweight.shape[0], wide - split), lambda i: (0, i))
    return pl.pallas_call(
        functools.partial(late_kernel, split),
        grid=(parts,),
        in_specs=[
            pl.BlockSpec((blocks, 1, rows, wide), lambda i: (0, i, 0, 0)),
            pl.BlockSpec(qbasis.shape, lambda i: (0, 0)),
            pl.BlockSpec(obasis.shape, lambda i: (0, 0)),
            qspec,
            ospec,
        ],
        out_specs=[qspec, ospec, qspec, ospec],
        out_shape=[
            jax.ShapeDtypeStruct(qweight.shape, F32),
            jax.ShapeDtypeStruct(oweight.shape, F32),
            jax.ShapeDtypeStruct(qweight.shape, BF16),
            jax.ShapeDtypeStruct(oweight.shape, BF16),
        ],
        name="late",
    )(dirs, qbasis, obasis, qweight, oweight)


def on_device(
    saved_latent,
    query_cotangent,
    mix_cotangent,
    head_outputs,
    query_weight,
    out_weight,
    query_basis,
    out_basis,
    query_mean,
    query_var,
    out_mean,
    out_var,
):
    blocks, parts, cores = (lax.axis_size(a) for a in ("fs", "rep", "tp"))
    owners = blocks * parts
    position = lax.axis_index("fs")
    query_rows, out_rows = query_weight.shape[0], out_weight.shape[0]
    query_local = lax.dynamic_slice_in_dim(query_basis, position * query_rows, query_rows, 0)
    out_local = lax.dynamic_slice_in_dim(out_basis, position * out_rows, out_rows, 0)
    split = query_cotangent.shape[1] // parts
    rank = query_basis.shape[1]
    counts = (
        float(rank * query_cotangent.shape[1] * cores),
        float(rank * head_outputs.shape[1] * cores),
    )
    terms = early(
        saved_latent, query_cotangent, mix_cotangent, head_outputs, query_basis, out_basis, blocks, parts
    )
    rows, wide = terms.shape[2:]
    sent = lax.all_to_all(terms.reshape(owners, rows, wide), ("fs", "rep"), 0, 0, tiled=True)
    proj, squares = total(sent, split, owners * cores)
    squares = lax.all_to_all(squares, ("fs", "rep", "tp"), 0, 0, tiled=True)
    mine = direction(
        squares, proj, query_mean, query_var, out_mean, out_var, split, counts, owners
    )
    dirs = lax.all_to_all(mine, ("fs", "rep"), 0, 0, tiled=True)
    dirs = dirs.reshape(blocks, parts, rows, wide)
    return tuple(late(dirs, query_local, out_local, query_weight, out_weight, split))


def solution(mesh):
    placed = (
        P(("fs", "rep"), None),
        P(("fs", "rep"), "tp"),
        P(("fs", "rep"), None),
        P(("fs", "rep"), "tp"),
        P("fs", "tp"),
        P("fs", "tp"),
        P(),
        P(),
        P("fs", "tp"),
        P("fs", "tp"),
        P("fs", "tp"),
        P("fs", "tp"),
    )
    return jax.shard_map(
        on_device,
        mesh=mesh,
        in_specs=placed,
        out_specs=(P("fs", "tp"), P("fs", "tp"), P("fs", "tp"), P("fs", "tp")),
        check_vma=False,
    )
```

time: 185 us -> 138 us (0.75)
  matrix products: 44.8 us -> 0 us
  Pallas kernels: 0 us -> 27.9 us
  between operations: 15.7 us -> 0.66 us
  other arithmetic: 10.5 us -> 0 us
  waiting for transfers between devices: 42.1 us -> 32.5 us
  starting transfers between devices: 0.04 us -> 5.17 us
  local copies, waits for them, and re-layouts: 4.27 us -> 8.78 us
  blocking collectives: 67.2 us -> 62.7 us
    dot_general x6 -> x0, matrix products: 44.8 us -> none  [the longest x2 23.9 us: project(): lax.dot_general(basis.astype(jnp.float32), grad, (((0,), (0,)), ((), ()))...]
    all_gather x1 -> x0, waiting for transfers between devices: 42.1 us -> none  [in_one_piece(): lax.all_gather(both, axis, axis=dim, tiled=True)]
    all_to_all x0 -> x1, waiting for transfers between devices: none -> 32.5 us  [on_device(): dirs = lax.all_to_all(mine, ('fs', 'rep'), 0, 0, tiled=True)]
    pallas_call x0 -> x4, Pallas kernels: none -> 27.9 us  [the longest x1 17 us: early(): pl.pallas_call(functools.partial(early_kernel, parts, rows), grid=(STEPS,...]
    unnamed x14 -> x8, local copies, waits for them, and re-layouts: 0.06 us -> 5.74 us
    all_to_all x0 -> x1, starting transfers between devices: none -> 5.17 us  [on_device(): dirs = lax.all_to_all(mine, ('fs', 'rep'), 0, 0, tiled=True)]
    reduce_sum x5 -> x0, other arithmetic: 4.86 us -> none  [the longest x1 1.88 us: sent_and_summed(): return jnp.sum(tiles, axis=0)]
    all_to_all x3 -> x2, blocking collectives: 67.2 us -> 62.7 us  [the longest x1 47.5 us: on_device(): lax.all_to_all(terms.reshape(owners, rows, wide), ('fs', 'rep'), 0, 0, ti...]
  transfers between devices with their start and end apart: 1 -> 1, of which waited for: 1 -> 1; matrix products, arithmetic and copies ran while one was open for 0% -> 2% of each run, Pallas kernels for 0% -> 0%
where the time goes in v1:
time: 138 us
  blocking collectives  62.7 us (45%)
  waiting for transfers between devices  32.5 us (24%)
  Pallas kernels  27.9 us (20%)
  local copies, waits for them, and re-layouts  8.78 us (6%)
  starting transfers between devices  5.17 us (4%)
    all_to_all x1, blocking collectives, on_device(): lax.all_to_all(terms.reshape(owners, rows, wide), ('fs', 'rep'), 0, 0, ti...  47.5 us
    all_to_all x1, waiting for transfers between devices, on_device(): dirs = lax.all_to_all(mine, ('fs', 'rep'), 0, 0, tiled=True)  32.5 us
    pallas_call x1, Pallas kernels, early(): pl.pallas_call(functools.partial(early_kernel, parts, rows), grid=(STEPS,...  17 us
    all_to_all x1, blocking collectives, on_device(): squares = lax.all_to_all(squares, ('fs', 'rep', 'tp'), 0, 0, tiled=True)  15.3 us
    unnamed x8, local copies, waits for them, and re-layouts  5.74 us
    all_to_all x1, starting transfers between devices, on_device(): dirs = lax.all_to_all(mine, ('fs', 'rep'), 0, 0, tiled=True)  5.17 us
    pallas_call x1, Pallas kernels, late(): pl.pallas_call(functools.partial(late_kernel, split), grid=(parts,), in_s...  4.74 us
    pallas_call x1, Pallas kernels, total(): pl.pallas_call(functools.partial(total_kernel, split, copies), grid=(4,),...  3.24 us
  transfers between devices with their start and end apart: 1, of which 1 were waited for; matrix products, arithmetic and copies ran while one was open for 2% of the time, Pallas kernels for 0%

profile of v1, /device:TPU:0, one launch (start us, length us, event | category | flops | bytes accessed | tf_op | source)
XLA Modules:
  0.0 137.8 jit_solution(17518028845084753063)
XLA Ops:
  0.6 0.0 copy-start
  0.6 1.6 %copy-done = bf16[4096,256]{1,0:T(8,128)(2,1)S(1)} copy-done((bf16[4096,256]{1,0:T(8,128)(2,1)S(1)}, bf16[4096,256]{1,0:T(8,128)(2,1)}, u32[]{:S(2)}) %copy-start) | copy-done | bytes 2097176
  2.2 0.0 copy-start.1
  2.2 1.4 %copy-done.1 = bf16[768,1024]{1,0:T(8,128)(2,1)S(1)} copy-done((bf16[768,1024]{1,0:T(8,128)(2,1)S(1)}, bf16[768,1024]{1,0:T(8,128)(2,1)}, u32[]{:S(2)}) %copy-start.1) | copy-done | bytes 1572888
  3.6 0.0 copy-start.2
  3.6 1.2 copy-done.2
  4.9 17.0 %early.1 = f32[16,4,16,640]{3,2,1,0:T(8,128)} custom-call(bf16[768,2048]{1,0:T(8,128)(2,1)} %latent.1, bf16[768,1536]{1,0:T(8,128)(2,1)} %cot.1, bf16[768,4096]{1,0:T(8,128)(2,1)} %mix.1, bf16[768,1024]{1,0:T(8,128)(2,1)S(1)} %copy-done.1, bf16[2048,256]{1,0:T(8,128)(2,1)S(1)} %copy-done.2, bf16[4096,256]{1,0:T(8,128)(2,1)S(1)} %copy-done), custom_call_target="tpu_custom_call" | custom-call | flops 4499999744 | bytes 19000000 | tf_op jit(solution)/shard_map/early/pallas_call | solution.py:56
  21.8 47.5 %all_to_all.15.terms = f32[64,16,640]{2,1,0:T(8,128)} all-to-all(f32[64,16,640]{2,1,0:T(8,128)} %bitcast.2), channel_id=1, replica_groups=mesh['fs'=16,'rep'=4,'tp'=2] {'fs','rep'}, dimensions={0} | all-to-all | bytes 5242880 | tf_op jit(solution)/shard_map/all_to_all | solution.py:206
  69.3 3.2 %total.1 = (f32[16,640]{1,0:T(8,128)}, f32[128,2,128]{2,1,0:T(2,128)}) custom-call(f32[64,16,640]{2,1,0:T(8,128)} %all_to_all.15.terms), custom_call_target="tpu_custom_call" | custom-call | tf_op jit(solution)/shard_map/total/pallas_call | solution.py:95
  72.5 15.3 %all_to_all.16.squares = f32[128,2,128]{2,1,0:T(2,128)} all-to-all(f32[128,2,128]{2,1,0:T(2,128)} %get-tuple-element.6), channel_id=1, replica_groups=mesh['fs'=16,'rep'=4,'tp'=2] {'fs','rep','tp'}, dimensions={0} | all-to-all | bytes 262144 | tf_op jit(solution)/shard_map/all_to_all | solution.py:208
  87.8 3.0 %direction.1 = f32[64,16,640]{2,1,0:T(8,128)} custom-call(f32[128,2,128]{2,1,0:T(2,128)} %all_to_all.16.squares, f32[16,640]{1,0:T(8,128)} %get-tuple-element.7.proj, f32[16,1536]{1,0:T(8,128)} %qmean.1, f32[16,1536]{1,0:T(8,128)} %qvar.1, f32[16,1024]{1,0:T(8,128)} %omean.1, f32[16,1024]{1,0:T(8,128)} %ovar.1), custom_call_target="tpu_custom_call" | custom-call | tf_op jit(solution)/shard_map/direction/pallas_call | solution.py:131
  90.8 5.2 %all-to-all-start.2 = ((f32[64,16,640]{2,1,0:T(8,128)}), f32[64,16,640]{2,1,0:T(8,128)S(1)}, u32[]{:S(2)}, u32[]{:S(2)}) async-start(f32[64,16,640]{2,1,0:T(8,128)} %direction.1), calls=%async_computation.2 | async-start | bytes 5242880 | tf_op jit(solution)/shard_map/all_to_all | solution.py:212
  96.0 1.5 %constant_dynamic-slice_fusion.1.qbasis = bf16[128,256]{1,0:T(8,128)(2,1)} fusion(bf16[2048,256]{1,0:T(8,128)(2,1)} %qbasis.1, s32[]{:T(128)S(6)} %select_n.6), kind=kLoop, calls=%fused_computation.1 | loop fusion | bytes 131076 | tf_op jit(solution)/shard_map/dynamic_slice | solution.py:194
  97.5 1.6 %constant_dynamic-slice_fusion.obasis = bf16[256,256]{1,0:T(8,128)(2,1)} fusion(bf16[4096,256]{1,0:T(8,128)(2,1)} %obasis.1, s32[]{:T(128)S(6)} %select_n.7), kind=kLoop, calls=%fused_computation | loop fusion | bytes 262148 | tf_op jit(solution)/shard_map/dynamic_slice | solution.py:195
  99.0 32.5 %all-to-all-done.2 = f32[64,16,640]{2,1,0:T(8,128)S(1)} async-done(((f32[64,16,640]{2,1,0:T(8,128)}), f32[64,16,640]{2,1,0:T(8,128)S(1)}, u32[]{:S(2)}, u32[]{:S(2)}) %all-to-all-start.2) | async-done | bytes 2621472 | tf_op jit(solution)/shard_map/all_to_all | solution.py:212
  131.5 0.0 copy-start.3
  131.5 1.5 %copy-done.3 = f32[64,16,640]{2,1,0:T(8,128)} copy-done((f32[64,16,640]{2,1,0:T(8,128)}, f32[64,16,640]{2,1,0:T(8,128)S(1)}, u32[]{:S(2)}) %copy-start.3) | copy-done | bytes 2621464
  133.0 4.7 %late.1 = (f32[128,1536]{1,0:T(8,128)}, f32[256,1024]{1,0:T(8,128)}, bf16[128,1536]{1,0:T(8,128)(2,1)}, bf16[256,1024]{1,0:T(8,128)(2,1)}) custom-call(f32[16,4,16,640]{3,2,1,0:T(8,128)} %bitcast.3, bf16[128,256]{1,0:T(8,128)(2,1)} %constant_dynamic-slice_fusion.1.qbasis, bf16[256,256]{1,0:T(8,128)(2,1)} %constant_dynamic-slice_fusion.obasis, ...), custom_call_target="tpu_custom_call" | custom-call | tf_op jit(solution)/shard_map/late/pallas_call | solution.py:155
Async XLA Ops:
  0.6 1.6 %copy-start = (bf16[4096,256]{1,0:T(8,128)(2,1)S(1)}, bf16[4096,256]{1,0:T(8,128)(2,1)}, u32[]{:S(2)}) copy-start(bf16[4096,256]{1,0:T(8,128)(2,1)} %obasis.1) | copy-start | bytes 6291460
  2.2 1.4 %copy-start.1 = (bf16[768,1024]{1,0:T(8,128)(2,1)S(1)}, bf16[768,1024]{1,0:T(8,128)(2,1)}, u32[]{:S(2)}) copy-start(bf16[768,1024]{1,0:T(8,128)(2,1)} %heads.1) | copy-start | bytes 4718596
  3.6 1.2 copy-start.2
  90.8 40.7 %all-to-all-start.2 = ((f32[64,16,640]{2,1,0:T(8,128)}), f32[64,16,640]{2,1,0:T(8,128)S(1)}, u32[]{:S(2)}, u32[]{:S(2)}) async-start(f32[64,16,640]{2,1,0:T(8,128)} %direction.1), calls=%async_computation.2 | async-start | bytes 5242880 | tf_op jit(solution)/shard_map/all_to_all | solution.py:212
  131.5 1.5 %copy-start.3 = (f32[64,16,640]{2,1,0:T(8,128)}, f32[64,16,640]{2,1,0:T(8,128)S(1)}, u32[]{:S(2)}) copy-start(f32[64,16,640]{2,1,0:T(8,128)S(1)} %all-to-all-done.2) | copy-start | bytes 7864324
